TPU v7x, 32 devices: a whole 2x2x4 slice. The times are simulated.
32 devices in a mesh: pp: 2 (over x), fs: 4 (over y, core), tp: 4 (over z).
Axes of the slice: x: 2, y: 2, z: 4, core: 2. Of those that a mesh axis runs over, the one named last changes fastest.
Arguments:
- inputs: bfloat16 [512, 2048], P('pp', ('fs', 'tp')), may hold values from -6 to 6
- norm_gain: bfloat16 [2, 2048], P('pp', ('fs', 'tp')), may hold values from 0.099609375 to 1.8984375
- w_value: bfloat16 [2, 2048, 2048], P('pp', None, ('fs', 'tp')), may hold values from -0.125 to 0.125
- w_gate: bfloat16 [2, 2048, 2048], P('pp', None, ('fs', 'tp')), may hold values from -0.125 to 0.125
- w_taps: bfloat16 [2, 31, 2048], P('pp', None, ('fs', 'tp')), may hold values from -1 to 1
- ln_gain: float32 [2, 2048], P('pp', ('fs', 'tp')), may hold values from 0.1 to 1.9
- ln_shift: float32 [2, 2048], P('pp', ('fs', 'tp')), may hold values from -3 to 3
Outputs:
- outputs: bfloat16 [512, 2048], P('pp', ('fs', 'tp'))
All inputs are finite; a program needn't handle non-finite values.
Results may differ from a plain program's by a relative error of at most 0.0085.
Values may be sent and summed in bfloat16 or wider, within the bound.
A program may use at most 64 MiB of HBM per device.

v0:
```python
import jax
import jax.numpy as jnp
from jax import lax
from jax.sharding import PartitionSpec as P

LEN = 128
norm_eps = 1e-06
layer_eps = 1e-05


def from_behind(block, axis, distance):
    devices = range(lax.axis_size(axis))
    route = [(i - distance, i) for i in devices if i - distance in devices]
    return lax.ppermute(block, axis, route)


def local(inputs, norm_gain, w_value, w_gate, w_taps, ln_gain, ln_shift):
    num_sections = lax.axis_size("pp")
    my_section = lax.axis_index("pp")
    model_width = w_value.shape[1]
    channels = w_value.shape[2]
    tap_count = w_taps.shape[1]
    fed_rows = lax.all_gather(inputs, "pp", axis=0, tiled=True)
    total_rows = fed_rows.shape[0]
    block_rows = LEN
    per_batch = LEN // block_rows
    block_count = total_rows // block_rows
    step_count = block_count + num_sections - 1
    gain_row = norm_gain[0]
    value_weight = w_value[0]
    gate_weight = w_gate[0]
    tap_weights = w_taps[0].astype(jnp.float32)
    layer_gain = ln_gain[0]
    layer_shift = ln_shift[0]

    def convolve(operands):
        history, gated_rows = operands
        padded = jnp.concatenate([history, gated_rows], axis=0)
        convolved = jnp.zeros((block_rows, channels), jnp.float32)
        for tap_index in range(tap_count):
            convolved = (
                convolved + padded[tap_index : tap_index + block_rows] * tap_weights[tap_index]
            )
        return convolved

    def skip_convolve(operands):
        return jnp.zeros((block_rows, channels), jnp.float32)

    def process_block(stream, history, active):
        stream_f = stream.astype(jnp.float32)
        zero_block = jnp.zeros((block_rows, channels), jnp.float32)
        squares = lax.psum(jnp.sum(stream_f * stream_f, axis=1), ("fs", "tp"))
        scale_rows = lax.rsqrt(squares / model_width + norm_eps)[:, None]
        normed = (stream_f * scale_rows * gain_row.astype(jnp.float32)).astype(jnp.bfloat16)
        shard_piece = lax.all_gather(normed, ("fs", "tp"), axis=1, tiled=True)

        def accumulate(current):
            return (
                jnp.dot(shard_piece, value_weight, preferred_element_type=jnp.float32),
                jnp.dot(shard_piece, gate_weight, preferred_element_type=jnp.float32),
            )

        def unchanged(current):
            return current

        value_sum, gate_sum = lax.cond(active, accumulate, unchanged, (zero_block, zero_block))
        gated_rows = value_sum * jax.nn.sigmoid(gate_sum)
        convolved = lax.cond(active, convolve, skip_convolve, (history, gated_rows))
        new_history = jnp.where(
            active, jnp.concatenate([history, gated_rows], axis=0)[block_rows:], history
        )
        moments = lax.psum(
            (jnp.sum(convolved, axis=1), jnp.sum(convolved * convolved, axis=1)), ("fs", "tp")
        )
        row_mean = moments[0][:, None] / model_width
        row_var = moments[1][:, None] / model_width - row_mean * row_mean
        normed_conv = (convolved - row_mean) * lax.rsqrt(
            row_var + layer_eps
        ) * layer_gain + layer_shift
        new_stream = (stream_f + jax.nn.silu(normed_conv)).astype(jnp.bfloat16)
        return (jnp.where(active, new_stream, stream), new_history)

    def step_body(step_index, loop_state):
        stream, history, results = loop_state
        block_index = step_index - my_section
        active = (block_index >= 0) & (block_index < block_count)
        safe_index = jnp.clip(block_index, 0, block_count - 1)
        row_offset = safe_index * block_rows
        first_rows = lax.dynamic_slice_in_dim(fed_rows, row_offset, block_rows, 0)
        stream = jnp.where(my_section == 0, first_rows, stream)
        history = jnp.where(
            active & (safe_index % per_batch == 0), jnp.zeros_like(history), history
        )
        new_stream, new_history = process_block(stream, history, active)
        previous = lax.dynamic_slice_in_dim(results, row_offset, block_rows, 0)
        keep_rows = active & (my_section == num_sections - 1)
        results = lax.dynamic_update_slice_in_dim(
            results, jnp.where(keep_rows, new_stream, previous), row_offset, 0
        )
        passed = from_behind(new_stream, "pp", 1)
        return (passed, new_history, results)

    initial = (
        jnp.zeros((block_rows, channels), jnp.bfloat16),
        jnp.zeros((tap_count - 1, channels), jnp.float32),
        jnp.zeros((total_rows, channels), jnp.bfloat16),
    )
    final_state = lax.fori_loop(0, step_count, step_body, initial)
    own_rows = inputs.shape[0]
    shares = final_state[2].reshape(num_sections, own_rows, channels)
    arrived = lax.all_to_all(shares, "pp", split_axis=0, concat_axis=0, tiled=True)
    return arrived[num_sections - 1]


def solution(mesh):
    in_specs = (
        P("pp", ("fs", "tp")),
        P("pp", ("fs", "tp")),
        P("pp", None, ("fs", "tp")),
        P("pp", None, ("fs", "tp")),
        P("pp", None, ("fs", "tp")),
        P("pp", ("fs", "tp")),
        P("pp", ("fs", "tp")),
    )
    out_specs = P("pp", ("fs", "tp"))
    return jax.shard_map(local, mesh=mesh, in_specs=in_specs, out_specs=out_specs, check_vma=False)
```

profile of v0, /device:TPU:0, one launch (start us, length us, event | category | flops | bytes accessed | tf_op | source)
XLA Modules:
  0.0 539.6 jit_solution(15302463253678728073)
XLA Ops:
  0.0 6.3 %all_gather.13 = bf16[512,128]{1,0:T(8,128)(2,1)S(1)} all-gather(bf16[256,128]{1,0:T(8,128)(2,1)} %param.13), channel_id=1, replica_groups=mesh['pp'=2,'fs'=4,'tp'=4] {'pp'}, dimensions={0}, use_global_device_ids=true | all-gather | bytes 196608 | tf_op jit(solution)/shard_map/all_gather | solution.py:23
  7.0 524.0 %while.20 = (s32[]{:T(128)}, bf16[128,128]{1,0:T(8,128)(2,1)S(1)}, f32[30,128]{1,0:T(8,128)S(1)}, bf16[512,128]{1,0:T(8,128)(2,1)S(1)}, s32[]{:T(128)}, /*index=...) while((s32[]{:T(128)}, bf16[128,128]{1,0:T(8,128)(2,1)S(1)}, ...), condition=%wide.region_11.12_spmd.clone, body=%wide.region_0.11_spmd.clone.sunk | while | flops 136179984 | bytes 5903558 | solution.py:108
  7.1 33.1 %psum.46 = f32[128]{0:T(128)S(1)} all-reduce(f32[128]{0:T(128)S(1)} %get-tuple-element.554), channel_id=1, replica_groups=mesh['pp'=2,'fs'=4,'tp'=4] {'fs','tp'}, use_global_device_ids=true, to_apply=%region_2.2 | all-reduce | flops 128 | bytes 1024 | tf_op jit(solution)/shard_map/while/body/eval_jaxpr/psum | solution.py:52
  40.3 33.2 %all_gather.16 = bf16[128,2048]{1,0:T(8,128)(2,1)S(1)} all-gather(bf16[128,128]{1,0:T(8,128)(2,1)S(1)} %fusion.106), channel_id=1, replica_groups=mesh['pp'=2,'fs'=4,'tp'=4] {'fs','tp'}, dimensions={1}, use_global_device_ids=true | all-gather | bytes 557056 | tf_op jit(solution)/shard_map/while/body/eval_jaxpr/all_gather | solution.py:55
  73.5 1.6 conditional.6
  75.6 31.4 %all-reduce.2 = (f32[128]{0:T(128)S(1)}, f32[128]{0:T(128)S(1)}) all-reduce(f32[128]{0:T(128)S(1)} %get-tuple-element.558, f32[128]{0:T(128)S(1)} %get-tuple-element.559), channel_id=1, replica_groups=mesh['pp'=2,'fs'=4,'tp'=4] {'fs','tp'}, use_global_device_ids=true, to_apply=%region_10.10 | all-reduce | flops 256 | bytes 2048 | tf_op jit(solution)/shard_map/while/body/eval_jaxpr/psum | solution.py:72
  107.1 1.7 collective-permute-start
  108.8 1.6 collective-permute-done
  110.5 30.2 %psum.46 = f32[128]{0:T(128)S(1)} all-reduce(f32[128]{0:T(128)S(1)} %get-tuple-element.554), channel_id=1, replica_groups=mesh['pp'=2,'fs'=4,'tp'=4] {'fs','tp'}, use_global_device_ids=true, to_apply=%region_2.2 | all-reduce | flops 128 | bytes 1024 | tf_op jit(solution)/shard_map/while/body/eval_jaxpr/psum | solution.py:52
  140.8 36.4 %all_gather.16 = bf16[128,2048]{1,0:T(8,128)(2,1)S(1)} all-gather(bf16[128,128]{1,0:T(8,128)(2,1)S(1)} %fusion.106), channel_id=1, replica_groups=mesh['pp'=2,'fs'=4,'tp'=4] {'fs','tp'}, dimensions={1}, use_global_device_ids=true | all-gather | bytes 557056 | tf_op jit(solution)/shard_map/while/body/eval_jaxpr/all_gather | solution.py:55
  177.2 1.6 conditional.6
  179.2 29.7 %all-reduce.2 = (f32[128]{0:T(128)S(1)}, f32[128]{0:T(128)S(1)}) all-reduce(f32[128]{0:T(128)S(1)} %get-tuple-element.558, f32[128]{0:T(128)S(1)} %get-tuple-element.559), channel_id=1, replica_groups=mesh['pp'=2,'fs'=4,'tp'=4] {'fs','tp'}, use_global_device_ids=true, to_apply=%region_10.10 | all-reduce | flops 256 | bytes 2048 | tf_op jit(solution)/shard_map/while/body/eval_jaxpr/psum | solution.py:72
  209.1 4.2 collective-permute-start
  213.3 1.6 collective-permute-done
  215.0 32.0 %psum.46 = f32[128]{0:T(128)S(1)} all-reduce(f32[128]{0:T(128)S(1)} %get-tuple-element.554), channel_id=1, replica_groups=mesh['pp'=2,'fs'=4,'tp'=4] {'fs','tp'}, use_global_device_ids=true, to_apply=%region_2.2 | all-reduce | flops 128 | bytes 1024 | tf_op jit(solution)/shard_map/while/body/eval_jaxpr/psum | solution.py:52
  247.1 33.5 %all_gather.16 = bf16[128,2048]{1,0:T(8,128)(2,1)S(1)} all-gather(bf16[128,128]{1,0:T(8,128)(2,1)S(1)} %fusion.106), channel_id=1, replica_groups=mesh['pp'=2,'fs'=4,'tp'=4] {'fs','tp'}, dimensions={1}, use_global_device_ids=true | all-gather | bytes 557056 | tf_op jit(solution)/shard_map/while/body/eval_jaxpr/all_gather | solution.py:55
  280.6 1.6 conditional.6
  282.7 32.0 %all-reduce.2 = (f32[128]{0:T(128)S(1)}, f32[128]{0:T(128)S(1)}) all-reduce(f32[128]{0:T(128)S(1)} %get-tuple-element.558, f32[128]{0:T(128)S(1)} %get-tuple-element.559), channel_id=1, replica_groups=mesh['pp'=2,'fs'=4,'tp'=4] {'fs','tp'}, use_global_device_ids=true, to_apply=%region_10.10 | all-reduce | flops 256 | bytes 2048 | tf_op jit(solution)/shard_map/while/body/eval_jaxpr/psum | solution.py:72
  314.8 4.2 collective-permute-start
  319.1 1.6 collective-permute-done
  320.8 29.8 %psum.46 = f32[128]{0:T(128)S(1)} all-reduce(f32[128]{0:T(128)S(1)} %get-tuple-element.554), channel_id=1, replica_groups=mesh['pp'=2,'fs'=4,'tp'=4] {'fs','tp'}, use_global_device_ids=true, to_apply=%region_2.2 | all-reduce | flops 128 | bytes 1024 | tf_op jit(solution)/shard_map/while/body/eval_jaxpr/psum | solution.py:52
  350.7 36.8 %all_gather.16 = bf16[128,2048]{1,0:T(8,128)(2,1)S(1)} all-gather(bf16[128,128]{1,0:T(8,128)(2,1)S(1)} %fusion.106), channel_id=1, replica_groups=mesh['pp'=2,'fs'=4,'tp'=4] {'fs','tp'}, dimensions={1}, use_global_device_ids=true | all-gather | bytes 557056 | tf_op jit(solution)/shard_map/while/body/eval_jaxpr/all_gather | solution.py:55
  387.5 1.6 conditional.6
  389.6 29.7 %all-reduce.2 = (f32[128]{0:T(128)S(1)}, f32[128]{0:T(128)S(1)}) all-reduce(f32[128]{0:T(128)S(1)} %get-tuple-element.558, f32[128]{0:T(128)S(1)} %get-tuple-element.559), channel_id=1, replica_groups=mesh['pp'=2,'fs'=4,'tp'=4] {'fs','tp'}, use_global_device_ids=true, to_apply=%region_10.10 | all-reduce | flops 256 | bytes 2048 | tf_op jit(solution)/shard_map/while/body/eval_jaxpr/psum | solution.py:72
  419.5 4.2 collective-permute-start
  423.7 1.6 collective-permute-done
  425.4 32.0 %psum.46 = f32[128]{0:T(128)S(1)} all-reduce(f32[128]{0:T(128)S(1)} %get-tuple-element.554), channel_id=1, replica_groups=mesh['pp'=2,'fs'=4,'tp'=4] {'fs','tp'}, use_global_device_ids=true, to_apply=%region_2.2 | all-reduce | flops 128 | bytes 1024 | tf_op jit(solution)/shard_map/while/body/eval_jaxpr/psum | solution.py:52
  457.5 33.3 %all_gather.16 = bf16[128,2048]{1,0:T(8,128)(2,1)S(1)} all-gather(bf16[128,128]{1,0:T(8,128)(2,1)S(1)} %fusion.106), channel_id=1, replica_groups=mesh['pp'=2,'fs'=4,'tp'=4] {'fs','tp'}, dimensions={1}, use_global_device_ids=true | all-gather | bytes 557056 | tf_op jit(solution)/shard_map/while/body/eval_jaxpr/all_gather | solution.py:55
  491.1 32.0 %all-reduce.2 = (f32[128]{0:T(128)S(1)}, f32[128]{0:T(128)S(1)}) all-reduce(f32[128]{0:T(128)S(1)} %get-tuple-element.558, f32[128]{0:T(128)S(1)} %get-tuple-element.559), channel_id=1, replica_groups=mesh['pp'=2,'fs'=4,'tp'=4] {'fs','tp'}, use_global_device_ids=true, to_apply=%region_10.10 | all-reduce | flops 256 | bytes 2048 | tf_op jit(solution)/shard_map/while/body/eval_jaxpr/psum | solution.py:72
  523.2 6.1 %collective-permute-start = (bf16[128,128]{1,0:T(8,128)(2,1)S(1)}, bf16[128,128]{1,0:T(8,128)(2,1)S(1)}, u32[]{:S(2)}, u32[]{:S(2)}) collective-permute-start(bf16[128,128]{1,0:T(8,128)(2,1)S(1)} %get-tuple-element.564), channel_id=1, source_target_pairs={{0,16},{1,17},{2,18},{3,19},{4,20},{5,21},{6,22},{7,23},{8,24},{9,... | collective-permute-start | bytes 98312 | tf_op jit(solution)/shard_map/while/body/eval_jaxpr/ppermute | solution.py:14
  529.3 1.7 collective-permute-done
  531.0 8.0 %all_to_all.5 = bf16[2,256,128]{2,1,0:T(8,128)(2,1)S(1)} all-to-all(bf16[2,256,128]{2,1,0:T(8,128)(2,1)S(1)} %bitcast.83), channel_id=1, replica_groups=mesh['pp'=2,'fs'=4,'tp'=4] {'pp'}, dimensions={0} | all-to-all | bytes 262144 | tf_op jit(solution)/shard_map/all_to_all | solution.py:111
  (97 shorter events, 12.5 us)
Async XLA Ops:
  0.0 6.3 %copy-start.3 = (bf16[1,31,128]{2,1,0:T(8,128)(2,1)S(1)}, bf16[1,31,128]{2,1,0:T(8,128)(2,1)}, u32[]{:S(2)}) copy-start(bf16[1,31,128]{2,1,0:T(8,128)(2,1)} %param.17) | copy-start | bytes 23812
  6.3 0.7 copy-start.1
  6.3 0.7 copy-start.2
  6.3 0.7 copy-start.4
  7.0 66.5 %copy-start = (bf16[2048,128]{1,0:T(8,128)(2,1)S(1)}, bf16[2048,128]{1,0:T(8,128)(2,1)}, u32[]{:S(2)}) copy-start(bf16[2048,128]{1,0:T(8,128)(2,1)} %get-tuple-element.619) | copy-start | bytes 1572868 | tf_op jit(solution)/shard_map/while
  107.1 3.2 collective-permute-start
  110.4 66.8 %copy-start = (bf16[2048,128]{1,0:T(8,128)(2,1)S(1)}, bf16[2048,128]{1,0:T(8,128)(2,1)}, u32[]{:S(2)}) copy-start(bf16[2048,128]{1,0:T(8,128)(2,1)} %get-tuple-element.619) | copy-start | bytes 1572868 | tf_op jit(solution)/shard_map/while
  209.1 5.8 %collective-permute-start = (bf16[128,128]{1,0:T(8,128)(2,1)S(1)}, bf16[128,128]{1,0:T(8,128)(2,1)S(1)}, u32[]{:S(2)}, u32[]{:S(2)}) collective-permute-start(bf16[128,128]{1,0:T(8,128)(2,1)S(1)} %get-tuple-element.564), channel_id=1, source_target_pairs={{0,16},{1,17},{2,18},{3,19},{4,20},{5,21},{6,22},{7,23},{8,24},{9,... | collective-permute-start | bytes 98312 | tf_op jit(solution)/shard_map/while/body/eval_jaxpr/ppermute | solution.py:14
  214.9 65.7 %copy-start = (bf16[2048,128]{1,0:T(8,128)(2,1)S(1)}, bf16[2048,128]{1,0:T(8,128)(2,1)}, u32[]{:S(2)}) copy-start(bf16[2048,128]{1,0:T(8,128)(2,1)} %get-tuple-element.619) | copy-start | bytes 1572868 | tf_op jit(solution)/shard_map/while
  314.8 5.8 %collective-permute-start = (bf16[128,128]{1,0:T(8,128)(2,1)S(1)}, bf16[128,128]{1,0:T(8,128)(2,1)S(1)}, u32[]{:S(2)}, u32[]{:S(2)}) collective-permute-start(bf16[128,128]{1,0:T(8,128)(2,1)S(1)} %get-tuple-element.564), channel_id=1, source_target_pairs={{0,16},{1,17},{2,18},{3,19},{4,20},{5,21},{6,22},{7,23},{8,24},{9,... | collective-permute-start | bytes 98312 | tf_op jit(solution)/shard_map/while/body/eval_jaxpr/ppermute | solution.py:14
  320.6 66.9 %copy-start = (bf16[2048,128]{1,0:T(8,128)(2,1)S(1)}, bf16[2048,128]{1,0:T(8,128)(2,1)}, u32[]{:S(2)}) copy-start(bf16[2048,128]{1,0:T(8,128)(2,1)} %get-tuple-element.619) | copy-start | bytes 1572868 | tf_op jit(solution)/shard_map/while
  419.5 5.8 %collective-permute-start = (bf16[128,128]{1,0:T(8,128)(2,1)S(1)}, bf16[128,128]{1,0:T(8,128)(2,1)S(1)}, u32[]{:S(2)}, u32[]{:S(2)}) collective-permute-start(bf16[128,128]{1,0:T(8,128)(2,1)S(1)} %get-tuple-element.564), channel_id=1, source_target_pairs={{0,16},{1,17},{2,18},{3,19},{4,20},{5,21},{6,22},{7,23},{8,24},{9,... | collective-permute-start | bytes 98312 | tf_op jit(solution)/shard_map/while/body/eval_jaxpr/ppermute | solution.py:14
  425.3 65.6 %copy-start = (bf16[2048,128]{1,0:T(8,128)(2,1)S(1)}, bf16[2048,128]{1,0:T(8,128)(2,1)}, u32[]{:S(2)}) copy-start(bf16[2048,128]{1,0:T(8,128)(2,1)} %get-tuple-element.619) | copy-start | bytes 1572868 | tf_op jit(solution)/shard_map/while
  523.2 7.8 %collective-permute-start = (bf16[128,128]{1,0:T(8,128)(2,1)S(1)}, bf16[128,128]{1,0:T(8,128)(2,1)S(1)}, u32[]{:S(2)}, u32[]{:S(2)}) collective-permute-start(bf16[128,128]{1,0:T(8,128)(2,1)S(1)} %get-tuple-element.564), channel_id=1, source_target_pairs={{0,16},{1,17},{2,18},{3,19},{4,20},{5,21},{6,22},{7,23},{8,24},{9,... | collective-permute-start | bytes 98312 | tf_op jit(solution)/shard_map/while/body/eval_jaxpr/ppermute | solution.py:14
where the time goes:
time: 540 us
  blocking collectives  499 us (92%)
  starting transfers between devices  20.4 us (4%)
  waiting for transfers between devices  8.02 us (1%)
  matrix products  6.45 us (1%)
    all_gather x5, blocking collectives, process_block(): shard_piece = lax.all_gather(normed, ('fs', 'tp'), axis=1, tiled=True)  173 us
    psum x5, blocking collectives, process_block(): squares = lax.psum(jnp.sum(stream_f * stream_f, axis=1), ('fs', 'tp'))  157 us
    psum x5, blocking collectives, process_block(): lax.psum((jnp.sum(convolved, axis=1), jnp.sum(convolved * convolved, axis...  155 us
    ppermute x5, starting transfers between devices, from_behind(): return lax.ppermute(block, axis, route)  20.4 us
  transfers between devices with their start and end apart: 5, of which 5 were waited for; matrix products, arithmetic and copies ran while one was open for 0% of the time, Pallas kernels for 0%

commit v1 on v0

--- a/solution.py
+++ b/solution.py
@@ -6,6 +6,11 @@
 LEN = 128
 norm_eps = 1e-06
 layer_eps = 1e-05
+
+
+def one_after_other(value, axis_one, axis_two):
+    half = lax.psum(value, axis_one)
+    return lax.psum(half, axis_two)
 
 
 def from_behind(block, axis, distance):
@@ -69,8 +74,8 @@
         new_history = jnp.where(
             active, jnp.concatenate([history, gated_rows], axis=0)[block_rows:], history
         )
-        moments = lax.psum(
-            (jnp.sum(convolved, axis=1), jnp.sum(convolved * convolved, axis=1)), ("fs", "tp")
+        moments = one_after_other(
+            (jnp.sum(convolved, axis=1), jnp.sum(convolved * convolved, axis=1)), "fs", "tp"
         )
         row_mean = moments[0][:, None] / model_width
         row_var = moments[1][:, None] / model_width - row_mean * row_mean

time: 540 us -> 462 us (0.86)
  blocking collectives: 499 us -> 421 us
    psum x5 -> x10, blocking collectives: 155 us -> 76.3 us  [the longest x5 47.9 us: one_after_other(): return lax.psum(half, axis_two)]
where the time goes in v1:
time: 462 us; the launch traced here: 461 us
  blocking collectives  421 us (91%)
  starting transfers between devices  20.3 us (4%)
  waiting for transfers between devices  7.87 us (2%)
  matrix products  6.46 us (1%)
    all_gather x5, blocking collectives, process_block(): shard_piece = lax.all_gather(normed, ('fs', 'tp'), axis=1, tiled=True)  174 us
    psum x5, blocking collectives, process_block(): squares = lax.psum(jnp.sum(stream_f * stream_f, axis=1), ('fs', 'tp'))  157 us
    psum x5, blocking collectives, one_after_other(): return lax.psum(half, axis_two)  47.9 us
    psum x5, blocking collectives, one_after_other(): half = lax.psum(value, axis_one)  28.3 us
    ppermute x5, starting transfers between devices, from_behind(): return lax.ppermute(block, axis, route)  20.3 us
  transfers between devices with their start and end apart: 5, of which 5 were waited for; matrix products, arithmetic and copies ran while one was open for 0% of the time, Pallas kernels for 0%

profile of v1, /device:TPU:0, one launch (start us, length us, event | category | flops | bytes accessed | tf_op | source)
XLA Modules:
  0.0 460.7 jit_solution(15233752507512994884)
XLA Ops:
  0.0 6.3 %all_gather.13 = bf16[512,128]{1,0:T(8,128)(2,1)S(1)} all-gather(bf16[256,128]{1,0:T(8,128)(2,1)} %param.13), channel_id=1, replica_groups=mesh['pp'=2,'fs'=4,'tp'=4] {'pp'}, dimensions={0}, use_global_device_ids=true | all-gather | bytes 196608 | tf_op jit(solution)/shard_map/all_gather | solution.py:28
  7.0 445.3 %while.20 = (s32[]{:T(128)}, bf16[128,128]{1,0:T(8,128)(2,1)S(1)}, f32[30,128]{1,0:T(8,128)S(1)}, bf16[512,128]{1,0:T(8,128)(2,1)S(1)}, s32[]{:T(128)}, /*index=...) while((s32[]{:T(128)}, bf16[128,128]{1,0:T(8,128)(2,1)S(1)}, ...), condition=%wide.region_13.14_spmd.clone, body=%wide.region_0.13_spmd.clone.sunk | while | flops 136180240 | bytes 5905606 | solution.py:113
  7.1 33.1 %psum.76 = f32[128]{0:T(128)S(1)} all-reduce(f32[128]{0:T(128)S(1)} %get-tuple-element.558), channel_id=1, replica_groups=mesh['pp'=2,'fs'=4,'tp'=4] {'fs','tp'}, use_global_device_ids=true, to_apply=%region_2.2 | all-reduce | flops 128 | bytes 1024 | tf_op jit(solution)/shard_map/while/body/eval_jaxpr/psum | solution.py:57
  40.3 33.2 %all_gather.16 = bf16[128,2048]{1,0:T(8,128)(2,1)S(1)} all-gather(bf16[128,128]{1,0:T(8,128)(2,1)S(1)} %fusion.106), channel_id=1, replica_groups=mesh['pp'=2,'fs'=4,'tp'=4] {'fs','tp'}, dimensions={1}, use_global_device_ids=true | all-gather | bytes 557056 | tf_op jit(solution)/shard_map/while/body/eval_jaxpr/all_gather | solution.py:60
  73.5 1.6 conditional.6
  75.6 5.7 %all-reduce.4 = (f32[128]{0:T(128)S(1)}, f32[128]{0:T(128)S(1)}) all-reduce(f32[128]{0:T(128)S(1)} %get-tuple-element.562, f32[128]{0:T(128)S(1)} %get-tuple-element.563), channel_id=1, replica_groups=mesh['pp'=2,'fs'=4,'tp'=4] {'fs'}, use_global_device_ids=true, to_apply=%region_11.11 | all-reduce | flops 256 | bytes 2048 | tf_op jit(solution)/shard_map/while/body/eval_jaxpr/psum | solution.py:12
  81.3 10.1 %all-reduce.5 = (f32[128]{0:T(128)S(1)}, f32[128]{0:T(128)S(1)}) all-reduce(f32[128]{0:T(128)S(1)} %get-tuple-element.564, f32[128]{0:T(128)S(1)} %get-tuple-element.565), channel_id=1, replica_groups=mesh['pp'=2,'fs'=4,'tp'=4] {'tp'}, use_global_device_ids=true, to_apply=%region_12.12 | all-reduce | flops 256 | bytes 2048 | tf_op jit(solution)/shard_map/while/body/eval_jaxpr/psum | solution.py:13
  91.6 1.6 collective-permute-start
  94.9 29.9 %psum.76 = f32[128]{0:T(128)S(1)} all-reduce(f32[128]{0:T(128)S(1)} %get-tuple-element.558), channel_id=1, replica_groups=mesh['pp'=2,'fs'=4,'tp'=4] {'fs','tp'}, use_global_device_ids=true, to_apply=%region_2.2 | all-reduce | flops 128 | bytes 1024 | tf_op jit(solution)/shard_map/while/body/eval_jaxpr/psum | solution.py:57
  124.8 36.9 %all_gather.16 = bf16[128,2048]{1,0:T(8,128)(2,1)S(1)} all-gather(bf16[128,128]{1,0:T(8,128)(2,1)S(1)} %fusion.106), channel_id=1, replica_groups=mesh['pp'=2,'fs'=4,'tp'=4] {'fs','tp'}, dimensions={1}, use_global_device_ids=true | all-gather | bytes 557056 | tf_op jit(solution)/shard_map/while/body/eval_jaxpr/all_gather | solution.py:60
  161.7 1.6 conditional.6
  163.8 5.7 %all-reduce.4 = (f32[128]{0:T(128)S(1)}, f32[128]{0:T(128)S(1)}) all-reduce(f32[128]{0:T(128)S(1)} %get-tuple-element.562, f32[128]{0:T(128)S(1)} %get-tuple-element.563), channel_id=1, replica_groups=mesh['pp'=2,'fs'=4,'tp'=4] {'fs'}, use_global_device_ids=true, to_apply=%region_11.11 | all-reduce | flops 256 | bytes 2048 | tf_op jit(solution)/shard_map/while/body/eval_jaxpr/psum | solution.py:12
  169.4 8.4 %all-reduce.5 = (f32[128]{0:T(128)S(1)}, f32[128]{0:T(128)S(1)}) all-reduce(f32[128]{0:T(128)S(1)} %get-tuple-element.564, f32[128]{0:T(128)S(1)} %get-tuple-element.565), channel_id=1, replica_groups=mesh['pp'=2,'fs'=4,'tp'=4] {'tp'}, use_global_device_ids=true, to_apply=%region_12.12 | all-reduce | flops 256 | bytes 2048 | tf_op jit(solution)/shard_map/while/body/eval_jaxpr/psum | solution.py:13
  178.0 4.2 collective-permute-start
  183.9 31.8 %psum.76 = f32[128]{0:T(128)S(1)} all-reduce(f32[128]{0:T(128)S(1)} %get-tuple-element.558), channel_id=1, replica_groups=mesh['pp'=2,'fs'=4,'tp'=4] {'fs','tp'}, use_global_device_ids=true, to_apply=%region_2.2 | all-reduce | flops 128 | bytes 1024 | tf_op jit(solution)/shard_map/while/body/eval_jaxpr/psum | solution.py:57
  215.8 33.5 %all_gather.16 = bf16[128,2048]{1,0:T(8,128)(2,1)S(1)} all-gather(bf16[128,128]{1,0:T(8,128)(2,1)S(1)} %fusion.106), channel_id=1, replica_groups=mesh['pp'=2,'fs'=4,'tp'=4] {'fs','tp'}, dimensions={1}, use_global_device_ids=true | all-gather | bytes 557056 | tf_op jit(solution)/shard_map/while/body/eval_jaxpr/all_gather | solution.py:60
  249.3 1.6 conditional.6
  251.4 5.7 %all-reduce.4 = (f32[128]{0:T(128)S(1)}, f32[128]{0:T(128)S(1)}) all-reduce(f32[128]{0:T(128)S(1)} %get-tuple-element.562, f32[128]{0:T(128)S(1)} %get-tuple-element.563), channel_id=1, replica_groups=mesh['pp'=2,'fs'=4,'tp'=4] {'fs'}, use_global_device_ids=true, to_apply=%region_11.11 | all-reduce | flops 256 | bytes 2048 | tf_op jit(solution)/shard_map/while/body/eval_jaxpr/psum | solution.py:12
  257.1 10.7 %all-reduce.5 = (f32[128]{0:T(128)S(1)}, f32[128]{0:T(128)S(1)}) all-reduce(f32[128]{0:T(128)S(1)} %get-tuple-element.564, f32[128]{0:T(128)S(1)} %get-tuple-element.565), channel_id=1, replica_groups=mesh['pp'=2,'fs'=4,'tp'=4] {'tp'}, use_global_device_ids=true, to_apply=%region_12.12 | all-reduce | flops 256 | bytes 2048 | tf_op jit(solution)/shard_map/while/body/eval_jaxpr/psum | solution.py:13
  267.9 4.2 collective-permute-start
  273.8 29.8 %psum.76 = f32[128]{0:T(128)S(1)} all-reduce(f32[128]{0:T(128)S(1)} %get-tuple-element.558), channel_id=1, replica_groups=mesh['pp'=2,'fs'=4,'tp'=4] {'fs','tp'}, use_global_device_ids=true, to_apply=%region_2.2 | all-reduce | flops 128 | bytes 1024 | tf_op jit(solution)/shard_map/while/body/eval_jaxpr/psum | solution.py:57
  303.7 36.5 %all_gather.16 = bf16[128,2048]{1,0:T(8,128)(2,1)S(1)} all-gather(bf16[128,128]{1,0:T(8,128)(2,1)S(1)} %fusion.106), channel_id=1, replica_groups=mesh['pp'=2,'fs'=4,'tp'=4] {'fs','tp'}, dimensions={1}, use_global_device_ids=true | all-gather | bytes 557056 | tf_op jit(solution)/shard_map/while/body/eval_jaxpr/all_gather | solution.py:60
  340.2 1.6 conditional.6
  342.3 5.7 %all-reduce.4 = (f32[128]{0:T(128)S(1)}, f32[128]{0:T(128)S(1)}) all-reduce(f32[128]{0:T(128)S(1)} %get-tuple-element.562, f32[128]{0:T(128)S(1)} %get-tuple-element.563), channel_id=1, replica_groups=mesh['pp'=2,'fs'=4,'tp'=4] {'fs'}, use_global_device_ids=true, to_apply=%region_11.11 | all-reduce | flops 256 | bytes 2048 | tf_op jit(solution)/shard_map/while/body/eval_jaxpr/psum | solution.py:12
  348.0 8.4 %all-reduce.5 = (f32[128]{0:T(128)S(1)}, f32[128]{0:T(128)S(1)}) all-reduce(f32[128]{0:T(128)S(1)} %get-tuple-element.564, f32[128]{0:T(128)S(1)} %get-tuple-element.565), channel_id=1, replica_groups=mesh['pp'=2,'fs'=4,'tp'=4] {'tp'}, use_global_device_ids=true, to_apply=%region_12.12 | all-reduce | flops 256 | bytes 2048 | tf_op jit(solution)/shard_map/while/body/eval_jaxpr/psum | solution.py:13
  356.5 4.2 collective-permute-start
  362.4 31.8 %psum.76 = f32[128]{0:T(128)S(1)} all-reduce(f32[128]{0:T(128)S(1)} %get-tuple-element.558), channel_id=1, replica_groups=mesh['pp'=2,'fs'=4,'tp'=4] {'fs','tp'}, use_global_device_ids=true, to_apply=%region_2.2 | all-reduce | flops 128 | bytes 1024 | tf_op jit(solution)/shard_map/while/body/eval_jaxpr/psum | solution.py:57
  394.4 33.8 %all_gather.16 = bf16[128,2048]{1,0:T(8,128)(2,1)S(1)} all-gather(bf16[128,128]{1,0:T(8,128)(2,1)S(1)} %fusion.106), channel_id=1, replica_groups=mesh['pp'=2,'fs'=4,'tp'=4] {'fs','tp'}, dimensions={1}, use_global_device_ids=true | all-gather | bytes 557056 | tf_op jit(solution)/shard_map/while/body/eval_jaxpr/all_gather | solution.py:60
  428.4 5.7 %all-reduce.4 = (f32[128]{0:T(128)S(1)}, f32[128]{0:T(128)S(1)}) all-reduce(f32[128]{0:T(128)S(1)} %get-tuple-element.562, f32[128]{0:T(128)S(1)} %get-tuple-element.563), channel_id=1, replica_groups=mesh['pp'=2,'fs'=4,'tp'=4] {'fs'}, use_global_device_ids=true, to_apply=%region_11.11 | all-reduce | flops 256 | bytes 2048 | tf_op jit(solution)/shard_map/while/body/eval_jaxpr/psum | solution.py:12
  434.0 10.4 %all-reduce.5 = (f32[128]{0:T(128)S(1)}, f32[128]{0:T(128)S(1)}) all-reduce(f32[128]{0:T(128)S(1)} %get-tuple-element.564, f32[128]{0:T(128)S(1)} %get-tuple-element.565), channel_id=1, replica_groups=mesh['pp'=2,'fs'=4,'tp'=4] {'tp'}, use_global_device_ids=true, to_apply=%region_12.12 | all-reduce | flops 256 | bytes 2048 | tf_op jit(solution)/shard_map/while/body/eval_jaxpr/psum | solution.py:13
  444.6 6.1 %collective-permute-start = (bf16[128,128]{1,0:T(8,128)(2,1)S(1)}, bf16[128,128]{1,0:T(8,128)(2,1)S(1)}, u32[]{:S(2)}, u32[]{:S(2)}) collective-permute-start(bf16[128,128]{1,0:T(8,128)(2,1)S(1)} %get-tuple-element.570), channel_id=1, source_target_pairs={{0,16},{1,17},{2,18},{3,19},{4,20},{5,21},{6,22},{7,23},{8,24},{9,... | collective-permute-start | bytes 98312 | tf_op jit(solution)/shard_map/while/body/eval_jaxpr/ppermute | solution.py:19
  452.3 7.8 %all_to_all.5 = bf16[2,256,128]{2,1,0:T(8,128)(2,1)S(1)} all-to-all(bf16[2,256,128]{2,1,0:T(8,128)(2,1)S(1)} %bitcast.83), channel_id=1, replica_groups=mesh['pp'=2,'fs'=4,'tp'=4] {'pp'}, dimensions={0} | all-to-all | bytes 262144 | tf_op jit(solution)/shard_map/all_to_all | solution.py:116
  (102 shorter events, 20.3 us)
Async XLA Ops:
  0.0 6.3 %copy-start.3 = (bf16[1,31,128]{2,1,0:T(8,128)(2,1)S(1)}, bf16[1,31,128]{2,1,0:T(8,128)(2,1)}, u32[]{:S(2)}) copy-start(bf16[1,31,128]{2,1,0:T(8,128)(2,1)} %param.17) | copy-start | bytes 23812
  6.3 0.7 copy-start.1
  6.3 0.7 copy-start.2
  6.3 0.7 copy-start.4
  7.0 66.5 %copy-start = (bf16[2048,128]{1,0:T(8,128)(2,1)S(1)}, bf16[2048,128]{1,0:T(8,128)(2,1)}, u32[]{:S(2)}) copy-start(bf16[2048,128]{1,0:T(8,128)(2,1)} %get-tuple-element.625) | copy-start | bytes 1572868 | tf_op jit(solution)/shard_map/while
  91.6 3.2 collective-permute-start
  94.7 67.0 %copy-start = (bf16[2048,128]{1,0:T(8,128)(2,1)S(1)}, bf16[2048,128]{1,0:T(8,128)(2,1)}, u32[]{:S(2)}) copy-start(bf16[2048,128]{1,0:T(8,128)(2,1)} %get-tuple-element.625) | copy-start | bytes 1572868 | tf_op jit(solution)/shard_map/while
  178.0 5.8 %collective-permute-start = (bf16[128,128]{1,0:T(8,128)(2,1)S(1)}, bf16[128,128]{1,0:T(8,128)(2,1)S(1)}, u32[]{:S(2)}, u32[]{:S(2)}) collective-permute-start(bf16[128,128]{1,0:T(8,128)(2,1)S(1)} %get-tuple-element.570), channel_id=1, source_target_pairs={{0,16},{1,17},{2,18},{3,19},{4,20},{5,21},{6,22},{7,23},{8,24},{9,... | collective-permute-start | bytes 98312 | tf_op jit(solution)/shard_map/while/body/eval_jaxpr/ppermute | solution.py:19
  183.8 65.5 %copy-start = (bf16[2048,128]{1,0:T(8,128)(2,1)S(1)}, bf16[2048,128]{1,0:T(8,128)(2,1)}, u32[]{:S(2)}) copy-start(bf16[2048,128]{1,0:T(8,128)(2,1)} %get-tuple-element.625) | copy-start | bytes 1572868 | tf_op jit(solution)/shard_map/while
  267.9 5.8 %collective-permute-start = (bf16[128,128]{1,0:T(8,128)(2,1)S(1)}, bf16[128,128]{1,0:T(8,128)(2,1)S(1)}, u32[]{:S(2)}, u32[]{:S(2)}) collective-permute-start(bf16[128,128]{1,0:T(8,128)(2,1)S(1)} %get-tuple-element.570), channel_id=1, source_target_pairs={{0,16},{1,17},{2,18},{3,19},{4,20},{5,21},{6,22},{7,23},{8,24},{9,... | collective-permute-start | bytes 98312 | tf_op jit(solution)/shard_map/while/body/eval_jaxpr/ppermute | solution.py:19
  273.7 66.6 %copy-start = (bf16[2048,128]{1,0:T(8,128)(2,1)S(1)}, bf16[2048,128]{1,0:T(8,128)(2,1)}, u32[]{:S(2)}) copy-start(bf16[2048,128]{1,0:T(8,128)(2,1)} %get-tuple-element.625) | copy-start | bytes 1572868 | tf_op jit(solution)/shard_map/while
  356.5 5.8 %collective-permute-start = (bf16[128,128]{1,0:T(8,128)(2,1)S(1)}, bf16[128,128]{1,0:T(8,128)(2,1)S(1)}, u32[]{:S(2)}, u32[]{:S(2)}) collective-permute-start(bf16[128,128]{1,0:T(8,128)(2,1)S(1)} %get-tuple-element.570), channel_id=1, source_target_pairs={{0,16},{1,17},{2,18},{3,19},{4,20},{5,21},{6,22},{7,23},{8,24},{9,... | collective-permute-start | bytes 98312 | tf_op jit(solution)/shard_map/while/body/eval_jaxpr/ppermute | solution.py:19
  362.3 65.8 %copy-start = (bf16[2048,128]{1,0:T(8,128)(2,1)S(1)}, bf16[2048,128]{1,0:T(8,128)(2,1)}, u32[]{:S(2)}) copy-start(bf16[2048,128]{1,0:T(8,128)(2,1)} %get-tuple-element.625) | copy-start | bytes 1572868 | tf_op jit(solution)/shard_map/while
  444.6 7.7 %collective-permute-start = (bf16[128,128]{1,0:T(8,128)(2,1)S(1)}, bf16[128,128]{1,0:T(8,128)(2,1)S(1)}, u32[]{:S(2)}, u32[]{:S(2)}) collective-permute-start(bf16[128,128]{1,0:T(8,128)(2,1)S(1)} %get-tuple-element.570), channel_id=1, source_target_pairs={{0,16},{1,17},{2,18},{3,19},{4,20},{5,21},{6,22},{7,23},{8,24},{9,... | collective-permute-start | bytes 98312 | tf_op jit(solution)/shard_map/while/body/eval_jaxpr/ppermute | solution.py:19
